TPU v7x, 32 devices: a whole 2x2x4 slice. The times are simulated.
32 devices in a mesh: sp: 16 (over z, y, core), tp: 2 (over x).
Axes of the slice: x: 2, y: 2, z: 4, core: 2. Of those that a mesh axis runs over, the one named last changes fastest.
Arguments:
- resid: bfloat16 [4096, 2048], P(('sp', 'tp')), may hold values from -6 to 6
- queries: bfloat16 [4096, 1024], P('sp', 'tp'), may hold values from -6 to 6
- keys: bfloat16 [512, 4096], P('tp', 'sp'), may hold values from -6 to 6
- values: bfloat16 [512, 4096], P('tp', 'sp'), may hold values from -6 to 6
- log_gates: float32 [16, 4096], P('tp', 'sp'), may hold values from -411 to 0, as said below
- q_gain: float32 [64], replicated, may hold values from 0.5 to 7
- k_gain: float32 [64], replicated, may hold values from 0.5 to 7
- w_out: bfloat16 [1024, 2048], P('tp'), may hold values from -0.1875 to 0.1875
- mlp_gain: bfloat16 [2048], replicated, may hold values from 0.099609375 to 1.8984375
- w_up: bfloat16 [2048, 8192], P('sp', 'tp'), may hold values from -0.125 to 0.125
- w_down: bfloat16 [8192, 2048], P('tp', 'sp'), may hold values from -0.0625 to 0.0625
Outputs:
- output: bfloat16 [4096, 2048], P(('sp', 'tp'))
Inputs may be any that keep to these rules, and one draw needn't show every extreme that they name: `log_gates`: each head's values never rise along positions.
All inputs are finite; a program needn't handle non-finite values.
Results may differ from a plain program's by a relative error of at most 0.018.
The roundings to bfloat16 on the way count: a program that leaves them out, or rounds other values in their place, can miss the bound.
Values may be sent and summed in bfloat16 or wider, within the bound.
A program may use at most 128 MiB of HBM per device.

v0:
```python
import math

import jax
import jax.numpy as jnp
from jax import lax
from jax.sharding import PartitionSpec as P

EPS = 1e-06


def rms_last(input_values, gain):
    scale = lax.rsqrt(jnp.mean(input_values * input_values, axis=-1, keepdims=True) + EPS)
    return input_values * scale * gain


def local(resid, queries, keys, values, log_gates, q_gain, k_gain, w_out, mlp_gain, w_up, w_down):
    up_whole, down_whole = (
        lax.all_gather(w_up, "sp", axis=0, tiled=True),
        lax.all_gather(w_down, "sp", axis=1, tiled=True),
    )
    positions = queries.shape[0]
    head_size = q_gain.shape[0]
    query_count = log_gates.shape[0]
    key_total_count = keys.shape[0] // head_size
    group = query_count // key_total_count
    query_heads = queries.astype(jnp.float32).reshape(positions, query_count, head_size)
    qnorm = (rms_last(query_heads, q_gain) * head_size ** (-0.5)).astype(jnp.bfloat16)
    qnorm = jnp.transpose(qnorm.reshape(positions, key_total_count, group, head_size), (1, 2, 0, 3))
    key_heads = keys.astype(jnp.float32).reshape(key_total_count, head_size, positions)
    key_scale = lax.rsqrt(jnp.mean(key_heads * key_heads, axis=1, keepdims=True) + EPS)
    knorm = (key_heads * key_scale * k_gain[None, :, None]).astype(jnp.bfloat16)
    knorm = knorm.reshape(key_total_count * head_size, positions)
    gates_all = lax.all_gather(log_gates, "sp", axis=1, tiled=True)
    offset = lax.axis_index("sp") * positions
    query_pos = offset + jnp.arange(positions, dtype=jnp.int32)
    query_last = offset + positions - 1
    query_gates = log_gates.reshape(key_total_count, group, positions)
    start_state = (
        jnp.full((key_total_count, group, positions), -1e30, jnp.float32),
        jnp.zeros((key_total_count, group, positions), jnp.float32),
        jnp.zeros((key_total_count, group, positions, head_size), jnp.float32),
    )
    key_piece = lax.all_gather(knorm, "sp", axis=1, tiled=True)
    value_piece = lax.all_gather(values, "sp", axis=1, tiled=True)
    length = key_piece.shape[1]
    block = math.gcd(length, 1024)
    key_blocks = key_piece.reshape(key_total_count, head_size, length)
    value_blocks = value_piece.reshape(key_total_count, head_size, length)

    def one_step(index, state):
        first = index * block

        def compute(inner):
            running_top, running_total, running_sum = inner
            key_now = lax.dynamic_slice_in_dim(key_blocks, index * block, block, 2)
            value_now = lax.dynamic_slice_in_dim(value_blocks, index * block, block, 2)
            gates_now = lax.dynamic_slice_in_dim(gates_all, first, block, 1).reshape(
                key_total_count, group, block
            )
            logits = jnp.einsum(
                "kgtd,kdn->kgtn", qnorm, key_now, preferred_element_type=jnp.float32
            )
            logits = logits + query_gates[..., None] - gates_now[:, :, None, :]
            key_pos = first + jnp.arange(block, dtype=jnp.int32)
            logits = jnp.where(key_pos[None, :] <= query_pos[:, None], logits, -jnp.inf)
            new_top = jnp.maximum(running_top, jnp.max(logits, axis=-1))
            rescale = jnp.exp(running_top - new_top)
            weights = jnp.exp(logits - new_top[..., None])
            new_total = running_total * rescale + jnp.sum(weights, axis=-1)
            product = jnp.einsum(
                "kgtn,kdn->kgtd",
                weights.astype(jnp.bfloat16),
                value_now,
                preferred_element_type=jnp.float32,
            )
            return (new_top, new_total, running_sum * rescale[..., None] + product)

        return lax.cond(first <= query_last, compute, lambda inner: inner, state)

    final_top, final_total, final_sum = lax.fori_loop(0, length // block, one_step, start_state)
    attn = final_sum / final_total[..., None]
    attn = (
        jnp.transpose(attn, (2, 0, 1, 3))
        .reshape(positions, query_count * head_size)
        .astype(jnp.bfloat16)
    )
    regrouped = lax.all_to_all(attn, "tp", split_axis=0, concat_axis=1, tiled=True)
    out_whole = lax.all_gather(w_out, "tp", axis=0, tiled=True)
    proj = jnp.dot(regrouped, out_whole, preferred_element_type=jnp.float32)
    mixed = (resid.astype(jnp.float32) + proj).astype(jnp.bfloat16)
    normed = rms_last(mixed.astype(jnp.float32), mlp_gain.astype(jnp.float32)).astype(jnp.bfloat16)
    upward = jnp.dot(
        lax.all_gather(normed, "tp", axis=0, tiled=True),
        up_whole,
        preferred_element_type=jnp.float32,
    )
    act = jnp.square(jax.nn.relu(upward)).astype(jnp.bfloat16)
    summed_down = lax.psum_scatter(
        jnp.dot(act, down_whole, preferred_element_type=jnp.float32).astype(jnp.bfloat16),
        "tp",
        scatter_dimension=0,
        tiled=True,
    ).astype(jnp.float32)
    return (mixed.astype(jnp.float32) + summed_down).astype(jnp.bfloat16)


def solution(mesh):
    return jax.shard_map(
        local,
        mesh=mesh,
        in_specs=(
            P(("sp", "tp"), None),
            P("sp", "tp"),
            P("tp", "sp"),
            P("tp", "sp"),
            P("tp", "sp"),
            P(),
            P(),
            P("tp", None),
            P(),
            P("sp", "tp"),
            P("tp", "sp"),
        ),
        out_specs=P(("sp", "tp"), None),
        check_vma=False,
    )
```

profile of v0, /device:TPU:0, one launch (start us, length us, event | category | flops | bytes accessed | tf_op | source)
XLA Modules:
  0.0 484.5 jit_solution(4621559039329992224)
XLA Ops:
  6.5 0.9 bitcast_reduce_fusion.1
  8.2 1.7 fusion.25
  11.4 1.1 copy.20
  12.6 23.8 %all_gather.22 = f32[8,4096]{1,0:T(8,128)S(1)} all-gather(f32[8,256]{1,0:T(8,128)} %param.19), channel_id=1, replica_groups=mesh['sp'=16,'tp'=2] {'sp'}, dimensions={1}, use_global_device_ids=true | all-gather | bytes 139264 | tf_op jit(solution)/shard_map/all_gather | solution.py:33
  36.4 0.8 fusion.26
  37.2 16.8 %all-gather.7.cloned.1.call-done = bf16[256,4096]{1,0:T(8,128)(2,1)} async-done(((bf16[256,256]{1,0:T(8,128)(2,1)}), bf16[256,4096]{1,0:T(8,128)(2,1)}) %all-gather.7.cloned.1.call-update) | async-done | bytes 2097168 | tf_op jit(solution)/shard_map/all_gather | solution.py:43
  53.9 42.3 %all-gather.9.cloned.1.call-done = bf16[256,4096]{1,0:T(8,128)(2,1)} async-done(((bf16[256,256]{1,0:T(8,128)(2,1)}), bf16[256,4096]{1,0:T(8,128)(2,1)}) %all-gather.9.cloned.1.call-update) | async-done | bytes 2097168 | tf_op jit(solution)/shard_map/all_gather | solution.py:44
  96.3 11.1 %while.18 = (s32[]{:T(128)}, f32[4,2,256]{2,1,0:T(2,128)S(1)}, f32[4,2,256]{2,1,0:T(2,128)S(1)}, f32[4,2,256,64]{2,3,1,0:T(8,128)S(1)}, s32[]{:T(128)}, /*index=...) while((s32[]{:T(128)}, f32[4,2,256]{2,1,0:T(2,128)S(1)}, ...), condition=%wide.region_7.8_spmd.clone, body=%wide.region_2.7_spmd.clone.sunk | while | flops 566760704 | bytes 28987796 | solution.py:80
  96.4 10.9 %conditional.3 = ((f32[4,2,256]{2,1,0:T(2,128)S(1)}, f32[4,2,256]{2,1,0:T(2,128)S(1)}, f32[4,2,256,64]{2,3,1,0:T(8,128)S(1)})) conditional(s32[]{:T(128)} %convert_element_type.114, (f32[4,2,256]{2,1,0:T(2,128)S(1)}, f32[4,2,256]{2,1,0:T(2,128)S(1)}, f32[4,2,256,64]{2,3,1,0:T(8,128)S(1)}) %tuple.46, (s32[]{:T(128)}, s32[]{:T(128)}, s32[]{:T(128)}, ...), branch_computations={%region_3.0_spmd, %region_4.6_spmd} | conditional | flops 566760704 | bytes 28986500 | solution.py:78
  97.4 3.6 fusion.5
  101.0 2.5 fusion.4
  103.6 3.7 fusion.9
  107.5 0.7 copy.21
  108.3 3.4 all-to-all-start
  111.8 9.1 %all-to-all-done = bf16[2,128,512]{1,2,0:T(8,128)(2,1)S(1)} async-done(((bf16[2,128,512]{1,2,0:T(8,128)(2,1)}), bf16[2,128,512]{1,2,0:T(8,128)(2,1)S(1)}, u32[]{:S(2)}, u32[]{:S(2)}) %all-to-all-start) | async-done | bytes 262176 | tf_op jit(solution)/shard_map/all_to_all | solution.py:87
  120.9 35.5 %all-gather.11.cloned.1.call-done = bf16[1024,2048]{1,0:T(8,128)(2,1)} async-done(((bf16[512,2048]{1,0:T(8,128)(2,1)}), bf16[1024,2048]{1,0:T(8,128)(2,1)}) %all-gather.11.cloned.1.call-update) | async-done | bytes 4194320 | tf_op jit(solution)/shard_map/all_gather | solution.py:88
  156.5 3.0 multiply_reduce_fusion
  159.5 1.0 multiply_convert_fusion
  161.7 20.2 %all-gather.13.cloned.1.call-done = bf16[256,2048]{1,0:T(8,128)(2,1)} async-done(((bf16[128,2048]{1,0:T(8,128)(2,1)}), bf16[256,2048]{1,0:T(8,128)(2,1)}) %all-gather.13.cloned.1.call-update) | async-done | bytes 1048592 | tf_op jit(solution)/shard_map/all_gather | solution.py:93
  181.9 128.5 %all-gather.15.cloned.1.call-done = bf16[2048,4096]{1,0:T(8,128)(2,1)} async-done(((bf16[128,4096]{1,0:T(8,128)(2,1)}), bf16[2048,4096]{1,0:T(8,128)(2,1)}) %all-gather.15.cloned.1.call-update) | async-done | bytes 16777232 | tf_op jit(solution)/shard_map/all_gather | solution.py:18
  310.4 130.1 %all-gather.17.cloned.1.call-done = bf16[4096,2048]{1,0:T(8,128)(2,1)} async-done(((bf16[4096,128]{1,0:T(8,128)(2,1)}), bf16[4096,2048]{1,0:T(8,128)(2,1)}) %all-gather.17.cloned.1.call-update) | async-done | bytes 16777232 | tf_op jit(solution)/shard_map/all_gather | solution.py:19
  440.5 16.5 %convolution_convert_fusion = bf16[256,2048]{1,0:T(8,128)(2,1)} fusion(bf16[4096,2048]{1,0:T(8,128)(2,1)} %all-gather.17.cloned.1.call-done, bf16[256,2048]{1,0:T(8,128)(2,1)} %all-gather.13.cloned.1.call-done, bf16[2048,4096]{1,0:T(8,128)(2,1)} %all-gather.15.cloned.1.call-done), kind=kOutput, calls=%fused_computation.27 | convolution fusion | flops 8593604608 | bytes 35651584 | tf_op jit(solution)/shard_map/dot_general | solution.py:99
  457.0 18.7 %reduce-scatter.2.cloned.1.call-done = bf16[128,2048]{1,0:T(8,128)(2,1)} async-done(((bf16[256,2048]{1,0:T(8,128)(2,1)}), bf16[128,2048]{1,0:T(8,128)(2,1)}) %reduce-scatter.2.cloned.1.call-update) | async-done | bytes 524304 | tf_op jit(solution)/shard_map/reduce_scatter | solution.py:98
  475.7 1.9 add_convert_fusion
  (47 shorter events, 4.8 us)
Async XLA Ops:
  6.5 47.4 %all-gather.7.cloned.1.call-start = ((), (), s32[]{:S(2)}) async-start(), calls=%async_computation.2 | async-start | bytes 2228224 | tf_op jit(solution)/shard_map/all_gather | solution.py:43
  9.9 86.3 %all-gather.9.cloned.1.call-start = ((), (), s32[]{:S(2)}) async-start(), calls=%async_computation.3 | async-start | bytes 2228224 | tf_op jit(solution)/shard_map/all_gather | solution.py:44
  10.7 145.8 %all-gather.11.cloned.1.call-start = ((), (), s32[]{:S(2)}) async-start(), calls=%async_computation.4 | async-start | bytes 6291456 | tf_op jit(solution)/shard_map/all_gather | solution.py:88
  96.3 15.5 %copy-start.1 = (bf16[2048]{0:T(1024)(128)(2,1)S(1)}, bf16[2048]{0:T(1024)(128)(2,1)}, u32[]{:S(2)}) copy-start(bf16[2048]{0:T(1024)(128)(2,1)} %param.23) | copy-start | bytes 12292
  96.3 60.1 %copy-start = (bf16[128,2048]{1,0:T(8,128)(2,1)S(1)}, bf16[128,2048]{1,0:T(8,128)(2,1)}, u32[]{:S(2)}) copy-start(bf16[128,2048]{1,0:T(8,128)(2,1)} %param.15) | copy-start | bytes 1572868
  108.3 12.6 %all-to-all-start = ((bf16[2,128,512]{1,2,0:T(8,128)(2,1)}), bf16[2,128,512]{1,2,0:T(8,128)(2,1)S(1)}, u32[]{:S(2)}, u32[]{:S(2)}) async-start(bf16[2,128,512]{1,2,0:T(8,128)(2,1)} %copy.21), calls=%async_computation | async-start | bytes 524288 | tf_op jit(solution)/shard_map/all_to_all | solution.py:87
  111.7 70.2 %all-gather.13.cloned.1.call-start = ((), (), s32[]{:S(2)}) async-start(), calls=%async_computation.5 | async-start | bytes 1572864 | tf_op jit(solution)/shard_map/all_gather | solution.py:93
  160.5 149.9 %all-gather.15.cloned.1.call-start = ((), (), s32[]{:S(2)}) async-start(), calls=%async_computation.6 | async-start | bytes 17825792 | tf_op jit(solution)/shard_map/all_gather | solution.py:18
  161.1 279.4 %all-gather.17.cloned.1.call-start = ((), (), s32[]{:S(2)}) async-start(), calls=%async_computation.7 | async-start | bytes 17825792 | tf_op jit(solution)/shard_map/all_gather | solution.py:19
  161.6 314.1 %reduce-scatter.2.cloned.1.call-start = ((), (), s32[]{:S(2)}) async-start(), calls=%async_computation.8 | async-start | bytes 1572864 | tf_op jit(solution)/shard_map/reduce_scatter | solution.py:98
Sparse Core Ops, SparseCore 0:
  10.0 43.8 all-gather.6
  56.1 40.1 all-gather.8
  97.8 58.5 all-gather.10
  160.6 21.2 all-gather.12
  183.9 126.4 all-gather.14
  312.4 128.0 all-gather.16
  457.1 18.5 reduce-scatter.1
where the time goes:
time: 485 us; the launch traced here: 484 us
  waiting for transfers between devices  404 us (83%)
  matrix products  26.8 us (6%)
  blocking collectives  23.8 us (5%)
  between operations  13.6 us (3%)
  other arithmetic  9.17 us (2%)
    all_gather x1, waiting for transfers between devices, local(): lax.all_gather(w_down, 'sp', axis=1, tiled=True)  130 us
    all_gather x1, waiting for transfers between devices, local(): lax.all_gather(w_up, 'sp', axis=0, tiled=True)  128 us
    all_gather x1, waiting for transfers between devices, local(): value_piece = lax.all_gather(values, 'sp', axis=1, tiled=True)  42.3 us
    all_gather x1, waiting for transfers between devices, local(): out_whole = lax.all_gather(w_out, 'tp', axis=0, tiled=True)  35.5 us
    all_gather x1, blocking collectives, local(): gates_all = lax.all_gather(log_gates, 'sp', axis=1, tiled=True)  23.8 us
    all_gather x1, waiting for transfers between devices, local(): lax.all_gather(normed, 'tp', axis=0, tiled=True)  20.2 us
    reduce_scatter x1, waiting for transfers between devices, local(): lax.psum_scatter(jnp.dot(act, down_whole, preferred_element_type=jnp.floa...  18.7 us
    all_gather x1, waiting for transfers between devices, local(): key_piece = lax.all_gather(knorm, 'sp', axis=1, tiled=True)  16.8 us
  transfers between devices with their start and end apart: 8, of which 8 were waited for; matrix products, arithmetic and copies ran while one was open for 3% of the time, Pallas kernels for 0%

commit v1 on v0

v1 whole, which is shorter than its diff:
```python
import functools
import math

import jax
import jax.numpy as jnp
from jax import lax
from jax.experimental import pallas as pl
from jax.experimental.pallas import tpu as pltpu
from jax.sharding import PartitionSpec as P


EPS = 1e-06
LANES = 128
BF = jnp.bfloat16
F32 = jnp.float32


def rms_last(input_values, gain):
    scale = lax.rsqrt(jnp.mean(input_values * input_values, axis=-1, keepdims=True) + EPS)
    return input_values * scale * gain


def split3(x):
    hi = lax.reduce_precision(x, 8, 7)
    mid = lax.reduce_precision(x - hi, 8, 7)
    low = lax.reduce_precision(x - hi - mid, 8, 7)
    return hi.astype(BF), mid.astype(BF), low.astype(BF)


def shifted(x, axis, delta):
    size = lax.axis_size(axis)
    return lax.ppermute(x, axis, [(i, (i + delta) % size) for i in range(size)])


def exchanged(x, axis, mask):
    size = lax.axis_size(axis)
    return lax.ppermute(x, axis, [(i, i ^ mask) for i in range(size)])


def ring_parts(x, axis, stride):
    count = lax.axis_size(axis) // stride
    rows = x.shape[0]
    out = [(0, 0, x)]
    forward = backward = x
    for step in range(1, (count - 1) // 2 + 1):
        forward = shifted(forward, axis, stride)
        backward = shifted(backward, axis, -stride)
        out += [(step, 0, forward), (count - step, 0, backward)]
    if count % 2 == 0:
        step = count // 2
        half = rows // 2 if count > 2 else rows
        out.append((step, 0, shifted(forward[:half], axis, stride)))
        if half < rows:
            out.append((step, half, shifted(backward[half:], axis, -stride)))
    return out


def attention_kernel(
    arrays, heads, group, head_size, positions, chunks, ids_ref, me_ref, q_ref, gate_ref, *refs
):
    pieces = refs[:arrays]
    out_ref, rhs_ref, top_ref, total_ref, sum_ref = refs[-5:]
    me = me_ref[0]
    top_ref[...] = jnp.full_like(top_ref, -1e30)
    total_ref[...] = jnp.zeros_like(total_ref)
    sum_ref[...] = jnp.zeros_like(sum_ref)
    width = group * positions
    value_rows = heads * head_size
    query_count = heads * group
    row = lax.broadcasted_iota(jnp.int32, (LANES, width), 0)
    column = lax.broadcasted_iota(jnp.int32, (LANES, width), 1) // positions
    for head in range(heads):
        picked = head * group + column
        pick = (row == picked) | (row == query_count + picked) | (row == 2 * query_count + picked)
        tail = jnp.where(pick, 1.0, 0.0)
        for part in range(3):
            gates = jnp.broadcast_to(gate_ref[head, part : part + 1, :], (LANES, width))
            tail = jnp.where(row == 3 * query_count + part, gates, tail)
        rhs_ref[head, :LANES, :] = jnp.zeros((LANES, width), BF)
        slot = head * head_size % LANES
        rhs_ref[head, slot : slot + head_size, :] = q_ref[head]
        rhs_ref[head, LANES:, :] = tail.astype(BF)

    def block(piece, index, masked):
        gates = piece[index, chunks * positions : (chunks + 1) * positions, :]
        base = (chunks + 1) * positions
        for head in range(heads):
            chunk = head * head_size // LANES
            lhs = jnp.concatenate(
                [piece[index, chunk * positions : (chunk + 1) * positions, :], gates], axis=1
            )
            logits = jnp.dot(lhs, rhs_ref[head], preferred_element_type=F32)
            if masked:
                key_pos = lax.broadcasted_iota(jnp.int32, (positions, width), 0)
                query_pos = lax.broadcasted_iota(jnp.int32, (positions, width), 1) % positions
                logits = jnp.where(key_pos <= query_pos, logits, -jnp.inf)
            old_top = top_ref[head]
            new_top = jnp.maximum(old_top, jnp.max(logits, axis=0, keepdims=True))
            rescale = jnp.exp(old_top - new_top)
            weights = jnp.exp(logits - new_top)
            total_ref[head] = total_ref[head] * rescale + jnp.sum(weights, axis=0, keepdims=True)
            top_ref[head] = new_top
            first = base + head * head_size
            value = jnp.concatenate(
                [
                    piece[index, first + c * value_rows : first + c * value_rows + head_size, :]
                    for c in range(positions // LANES)
                ],
                axis=1,
            )
            sum_ref[head] = sum_ref[head] * rescale + jnp.dot(
                value, weights.astype(BF), preferred_element_type=F32
            )

    block(pieces[0], 0, True)
    per = pieces[0].shape[0]
    for number in range(arrays):

        def body(index, carry, number=number):
            @pl.when(ids_ref[number * per + index] < me)
            def _():
                block(pieces[number], index, False)

            return carry

        lax.fori_loop(0, per, body, 0)
    for head in range(heads):
        result = sum_ref[head] / total_ref[head]
        for g in range(group):
            first = (head * group + g) * head_size
            out_ref[first : first + head_size, :] = result[
                :, g * positions : (g + 1) * positions
            ].astype(BF)


def hidden_units(rows, up_whole):
    product = jnp.dot(rows, up_whole, preferred_element_type=F32)
    return jnp.square(jax.nn.relu(product)).astype(BF)


def square_tail(own, up_whole, groups):
    rows, half = own.shape[0], own.shape[0] // 2

    def swap(x, mask):
        return exchanged(x, "sp", mask) if mask else exchanged(x, "tp", 1)

    side, across = swap(own, 0), swap(own, 2)
    corner_first, corner_last = swap(across[:half], 0), swap(side[half:], 2)
    mine = [own, side, across, corner_first, corner_last]
    mine_act = hidden_units(jnp.concatenate(mine, axis=0), up_whole)
    other_rows = jnp.concatenate([swap(part, 1) for part in mine], axis=0)
    other_act = hidden_units(other_rows, up_whole)
    cuts = [(3 * rows, 4 * rows), (rows, 3 * rows), (0, rows)]
    out = []
    for weight in groups:
        other = jnp.dot(other_act, weight, preferred_element_type=F32).astype(BF)
        partial = jnp.dot(mine_act, weight, preferred_element_type=F32)
        corner_in, middle_in, own_in = [swap(other[a:b], 1).astype(F32) for a, b in cuts]
        corner = (partial[3 * rows :] + corner_in).astype(BF)
        middle = partial[rows : 3 * rows] + middle_in
        from_across = swap(corner[:half], 2).astype(F32)
        from_side = swap(corner[half:], 0).astype(F32)
        side_sum = jnp.concatenate([middle[:half] + from_across, middle[half:rows]], axis=0)
        across_sum = jnp.concatenate([middle[rows:-half], middle[-half:] + from_side], axis=0)
        side_out = swap(side_sum.astype(BF), 0).astype(F32)
        across_out = swap(across_sum.astype(BF), 2).astype(F32)
        out.append(partial[:rows] + own_in + side_out + across_out)
    return out


def general_tail(normed, up_whole, down_whole, inner, tp):
    share = normed.shape[0]
    rows_all = jnp.concatenate(
        [normed] + [shifted(normed, "tp", step) for step in range(1, tp)], axis=0
    )
    bit = inner // 2
    while bit:
        rows_all = jnp.concatenate([rows_all, exchanged(rows_all, "sp", bit)], axis=0)
        bit //= 2
    act = hidden_units(rows_all, up_whole)
    partial = jnp.dot(act, down_whole, preferred_element_type=F32)
    bit = 1
    while bit < inner:
        half = partial.shape[0] // 2
        partial = partial[:half] + exchanged(partial[half:].astype(BF), "sp", bit).astype(F32)
        bit *= 2
    total = partial[:share]
    for step in range(1, tp):
        block = partial[step * share : (step + 1) * share].astype(BF)
        total = total + shifted(block, "tp", -step).astype(F32)
    return total


def local(resid, queries, keys, values, log_gates, q_gain, k_gain, w_out, mlp_gain, w_up, w_down):
    sp, tp = lax.axis_size("sp"), lax.axis_size("tp")
    me, my_tp = lax.axis_index("sp"), lax.axis_index("tp")
    inner = math.gcd(sp, 4)
    outer = sp // inner
    my_inner, my_outer = me % inner, me // inner
    positions = queries.shape[0]
    head_size = q_gain.shape[0]
    query_count = log_gates.shape[0]
    heads = keys.shape[0] // head_size
    group = query_count // heads

    key_heads = keys.astype(F32).reshape(heads, head_size, positions)
    key_scale = lax.rsqrt(jnp.mean(key_heads * key_heads, axis=1, keepdims=True) + EPS)
    knorm = (key_heads * key_scale * k_gain[None, :, None]).astype(BF)
    knorm = knorm.reshape(heads * head_size, positions).T
    chunks = -(-heads * head_size // LANES)
    knorm = jnp.pad(knorm, ((0, 0), (0, chunks * LANES - heads * head_size)))
    gate_parts = split3(log_gates)
    gate_block = jnp.concatenate(
        [-part.T for part in gate_parts]
        + [jnp.ones((positions, 3), BF), jnp.zeros((positions, LANES - 3 * query_count - 3), BF)],
        axis=1,
    )
    packed = jnp.concatenate(
        [knorm[:, c * LANES : (c + 1) * LANES] for c in range(chunks)]
        + [gate_block]
        + [values[:, c * LANES : (c + 1) * LANES] for c in range(positions // LANES)],
        axis=0,
    )
    rows = packed.shape[0]
    ring = sorted(ring_parts(packed, "sp", inner), key=lambda part: part[:2])
    stacked = jnp.concatenate([part[2] for part in ring], axis=0).reshape(outer, rows, LANES)
    arrays, masks = [stacked], [0]
    bit = inner // 2
    while bit:
        arrays += [exchanged(a, "sp", bit) for a in arrays]
        masks += [mask ^ bit for mask in masks]
        bit //= 2
    back = jnp.arange(outer, dtype=jnp.int32)
    ids = jnp.concatenate(
        [((my_outer - back) % outer) * inner + (my_inner ^ mask) for mask in masks]
    ).astype(jnp.int32)

    hidden = w_up.shape[1] // inner
    depth = w_up.shape[0]

    def spread(piece_for, axis):
        own = piece_for(my_inner)
        size = own.shape[axis]
        shape = list(own.shape)
        shape[axis] *= inner
        whole = jnp.zeros(shape, BF)
        whole = lax.dynamic_update_slice_in_dim(whole, own, my_inner * size, axis)
        for mask in range(1, inner):
            got = exchanged(piece_for(my_inner ^ mask), "sp", mask)
            whole = lax.dynamic_update_slice_in_dim(whole, got, (my_inner ^ mask) * size, axis)
        return whole

    up_part = spread(lambda e: lax.dynamic_slice_in_dim(w_up, e * hidden, hidden, 1), 0)
    down_part = spread(lambda e: lax.dynamic_slice_in_dim(w_down, e * hidden, hidden, 0), 1)
    up_ring = ring_parts(up_part, "sp", inner)
    down_ring = ring_parts(down_part, "sp", inner)
    early = [part for _, _, part in up_ring[1:3]]

    query_heads = queries.astype(F32).reshape(positions, query_count, head_size)
    qnorm = (rms_last(query_heads, q_gain) * head_size ** (-0.5)).astype(BF)
    qt = jnp.transpose(qnorm.reshape(positions, heads, group, head_size), (1, 3, 2, 0))
    qt = qt.reshape(heads, head_size, group * positions)
    own_gates = jnp.stack([part.astype(F32) for part in gate_parts], axis=1)
    own_gates = own_gates.reshape(heads, group, 3, positions).transpose(0, 2, 1, 3)
    own_gates = own_gates.reshape(heads, 3, group * positions)

    smem = pl.BlockSpec(memory_space=pltpu.SMEM)
    vmem = pl.BlockSpec(memory_space=pltpu.VMEM)
    width = group * positions
    attn = pl.pallas_call(
        functools.partial(
            attention_kernel, len(arrays), heads, group, head_size, positions, chunks
        ),
        out_shape=jax.ShapeDtypeStruct((query_count * head_size, positions), BF),
        in_specs=[smem, smem, vmem, vmem] + [vmem] * len(arrays)
        + [pl.BlockSpec(memory_space=pl.ANY)] * len(early),
        out_specs=vmem,
        scratch_shapes=[
            pltpu.VMEM((heads, 2 * LANES, width), BF),
            pltpu.VMEM((heads, 1, width), F32),
            pltpu.VMEM((heads, 1, width), F32),
            pltpu.VMEM((heads, head_size, width), F32),
        ],
        compiler_params=pltpu.CompilerParams(vmem_limit_bytes=40 * 1024 * 1024),
        cost_estimate=pl.CostEstimate(
            flops=6 * sp * heads * width * positions * LANES,
            bytes_accessed=2 * sp * rows * LANES,
            transcendentals=sp * heads * width * positions,
        ),
    )(ids, me.astype(jnp.int32).reshape(1), qt, own_gates, *arrays, *early)

    up_whole = jnp.zeros((depth * sp, hidden), BF)
    for step, first, part in up_ring:
        start = ((my_outer - step) % outer) * up_part.shape[0] + first
        up_whole = lax.dynamic_update_slice(up_whole, part, (start, 0))
    share = positions // tp
    proj = jnp.zeros((share, resid.shape[1]), F32)
    weight = w_out
    for step in range(tp):
        target = (my_tp + step) % tp
        mine = lax.dynamic_slice_in_dim(attn, target * share, share, 1)
        if step:
            mine = shifted(mine, "tp", step)
            weight = shifted(weight, "tp", 1)
        proj = proj + lax.dot_general(
            mine, weight, (((0,), (0,)), ((), ())), preferred_element_type=F32
        )
    mixed = (resid.astype(F32) + proj).astype(BF)
    normed = rms_last(mixed.astype(F32), mlp_gain.astype(F32)).astype(BF)

    if tp == 2 and inner == 4:
        by_step = {}
        for step, first, part in down_ring:
            by_step.setdefault(step, []).append(part)
        last = outer // 2
        steps = [step for step in by_step if step != last]
        whole = {step: jnp.concatenate(parts, axis=0) for step, parts in by_step.items()}
        groups = [jnp.concatenate([whole[step] for step in steps], axis=1), whole[last]]
        wide = whole[last].shape[1]
        totals = square_tail(normed, up_whole, groups)
        total = jnp.zeros(mixed.shape, F32)
        for number, step in enumerate(steps + [last]):
            start = ((my_outer - step) % outer) * wide
            piece = totals[1] if step == last else totals[0][:, number * wide : (number + 1) * wide]
            total = lax.dynamic_update_slice_in_dim(total, piece, start, 1)
    else:
        down_whole = jnp.zeros((hidden, depth * sp), BF)
        for step, first, part in down_ring:
            start = ((my_outer - step) % outer) * down_part.shape[1]
            down_whole = lax.dynamic_update_slice(down_whole, part, (first, start))
        total = general_tail(normed, up_whole, down_whole, inner, tp)
    return (mixed.astype(F32) + total).astype(BF)


def solution(mesh):
    return jax.shard_map(
        local,
        mesh=mesh,
        in_specs=(
            P(("sp", "tp"), None),
            P("sp", "tp"),
            P("tp", "sp"),
            P("tp", "sp"),
            P("tp", "sp"),
            P(),
            P(),
            P("tp", None),
            P(),
            P("sp", "tp"),
            P("tp", "sp"),
        ),
        out_specs=P(("sp", "tp"), None),
        check_vma=False,
    )
```

time: 485 us -> 284 us (0.59)
  waiting for transfers between devices: 404 us -> 167 us
  starting transfers between devices: 3.69 us -> 63.7 us
  blocking collectives: 23.8 us -> 0 us
  local copies, waits for them, and re-layouts: 3.45 us -> 25.3 us
  between operations: 13.6 us -> 0.76 us
  matrix products: 26.8 us -> 15.4 us
    all_gather x6 -> x0, waiting for transfers between devices: 373 us -> none  [the longest x1 130 us: local(): lax.all_gather(w_down, 'sp', axis=1, tiled=True)]
    ppermute x0 -> x46, waiting for transfers between devices: none -> 167 us  [the longest x14 89.5 us: shifted(): return lax.ppermute(x, axis, [(i, (i + delta) % size) for i in range(size)])]
    ppermute x0 -> x46, starting transfers between devices: none -> 63.7 us  [the longest x14 40.4 us: shifted(): return lax.ppermute(x, axis, [(i, (i + delta) % size) for i in range(size)])]
    all_gather x1 -> x0, blocking collectives: 23.8 us -> none  [local(): gates_all = lax.all_gather(log_gates, 'sp', axis=1, tiled=True)]
    reduce_scatter x1 -> x0, waiting for transfers between devices: 18.7 us -> none  [local(): lax.psum_scatter(jnp.dot(act, down_whole, preferred_element_type=jnp.floa...]
    dot_general x4 -> x8, matrix products: 26.8 us -> 15.4 us  [the longest x2 4.72 us: hidden_units(): product = jnp.dot(rows, up_whole, preferred_element_type=F32)]
    all_to_all x1 -> x0, waiting for transfers between devices: 9.1 us -> none  [local(): lax.all_to_all(attn, 'tp', split_axis=0, concat_axis=1, tiled=True)]
    dynamic_update_slice x0 -> x14, local copies, waits for them, and re-layouts: none -> 8.96 us  [the longest x6 7.25 us: spread(): lax.dynamic_update_slice_in_dim(whole, got, (my_inner ^ mask) * size, axis)]
  transfers between devices with their start and end apart: 8 -> 46, of which waited for: 8 -> 25; matrix products, arithmetic and copies ran while one was open for 3% -> 12% of each run, Pallas kernels for 0% -> 1%
where the time goes in v1:
time: 284 us; the launch traced here: 283 us
  waiting for transfers between devices  167 us (59%)
  starting transfers between devices  63.7 us (22%)
  local copies, waits for them, and re-layouts  25.3 us (9%)
  matrix products  15.4 us (5%)
  other arithmetic  6.96 us (2%)
  Pallas kernels  4.12 us (1%)
    ppermute x14, waiting for transfers between devices, shifted(): return lax.ppermute(x, axis, [(i, (i + delta) % size) for i in range(size)])  89.5 us
    ppermute x32, waiting for transfers between devices, exchanged(): return lax.ppermute(x, axis, [(i, i ^ mask) for i in range(size)])  77.6 us
    ppermute x14, starting transfers between devices, shifted(): return lax.ppermute(x, axis, [(i, (i + delta) % size) for i in range(size)])  40.4 us
    ppermute x32, starting transfers between devices, exchanged(): return lax.ppermute(x, axis, [(i, i ^ mask) for i in range(size)])  23.3 us
    dynamic_update_slice x6, local copies, waits for them, and re-layouts, spread(): lax.dynamic_update_slice_in_dim(whole, got, (my_inner ^ mask) * size, axis)  7.25 us
    unnamed x39, local copies, waits for them, and re-layouts  5.93 us
  transfers between devices with their start and end apart: 46, of which 25 were waited for; matrix products, arithmetic and copies ran while one was open for 12% of the time, Pallas kernels for 1%

profile of v1, /device:TPU:0, one launch (start us, length us, event | category | flops | bytes accessed | tf_op | source)
XLA Modules:
  0.0 283.3 jit_solution(3931885054243296401)
XLA Ops:
  8.1 3.1 %collective-permute-start = (bf16[1280,128]{0,1:T(8,128)(2,1)}, bf16[1280,128]{0,1:T(8,128)(2,1)S(1)}, u32[]{:S(2)}, u32[]{:S(2)}) collective-permute-start(bf16[1280,128]{0,1:T(8,128)(2,1)} %get-tuple-element.45), channel_id=1, source_target_pairs={{0,8},{2,10},{4,12},{6,14},{8,16},{10,18},{12,20},{14,22},{16,24},... | collective-permute-start | bytes 983048 | tf_op jit(solution)/shard_map/ppermute | solution.py:32
  15.2 6.8 %collective-permute-done = bf16[1280,128]{0,1:T(8,128)(2,1)S(1)} collective-permute-done((bf16[1280,128]{0,1:T(8,128)(2,1)}, bf16[1280,128]{0,1:T(8,128)(2,1)S(1)}, u32[]{:S(2)}, u32[]{:S(2)}) %collective-permute-start) | collective-permute-done | bytes 327712 | tf_op jit(solution)/shard_map/ppermute | solution.py:32
  22.1 5.7 %collective-permute-done.2 = bf16[1280,128]{0,1:T(8,128)(2,1)S(1)} collective-permute-done((bf16[1280,128]{0,1:T(8,128)(2,1)}, bf16[1280,128]{0,1:T(8,128)(2,1)S(1)}, u32[]{:S(2)}, u32[]{:S(2)}) %collective-permute-start.2) | collective-permute-done | bytes 327712 | tf_op jit(solution)/shard_map/ppermute | solution.py:32
  27.8 3.1 %collective-permute-start.3 = (bf16[640,128]{0,1:T(8,128)(2,1)S(1)}, bf16[640,128]{0,1:T(8,128)(2,1)S(1)}, u32[]{:S(2)}, u32[]{:S(2)}) collective-permute-start(bf16[640,128]{0,1:T(8,128)(2,1)S(1)} %slice.163), channel_id=1, source_target_pairs={{0,24},{2,26},{4,28},{6,30},{8,0},{10,2},{12,4},{14,6},{16,8},{18,... | collective-permute-start | bytes 491528 | tf_op jit(solution)/shard_map/ppermute | solution.py:32
  31.0 2.8 collective-permute-done.1
  40.9 32.9 %collective-permute-done.8 = bf16[128,1024]{1,0:T(8,128)(2,1)S(1)} collective-permute-done((bf16[128,1024]{1,0:T(8,128)(2,1)S(1)}, bf16[128,1024]{1,0:T(8,128)(2,1)S(1)}, u32[]{:S(2)}, u32[]{:S(2)}) %collective-permute-start.8) | collective-permute-done | bytes 262176 | tf_op jit(solution)/shard_map/ppermute | solution.py:37
  74.5 2.7 collective-permute-done.9
  79.3 2.4 collective-permute-start.11
  88.6 4.6 %collective-permute-done.21 = bf16[1024,128]{1,0:T(8,128)(2,1)} collective-permute-done((bf16[1024,128]{1,0:T(8,128)(2,1)}, bf16[1024,128]{1,0:T(8,128)(2,1)}, u32[]{:S(2)}, u32[]{:S(2)}) %collective-permute-start.21) | collective-permute-done | bytes 262176 | tf_op jit(solution)/shard_map/ppermute | solution.py:37
  95.4 2.5 collective-permute-done.22
  102.6 3.4 %collective-permute-done.10.refs_4_ = bf16[512,1024]{1,0:T(8,128)(2,1)S(1)} collective-permute-done((bf16[512,1024]{1,0:T(8,128)(2,1)}, bf16[512,1024]{1,0:T(8,128)(2,1)S(1)}, u32[]{:S(2)}, u32[]{:S(2)}) %collective-permute-start.10) | collective-permute-done | bytes 1048608 | tf_op jit(solution)/shard_map/ppermute | solution.py:32
  106.0 21.4 %collective-permute-done.11.refs_5_ = bf16[512,1024]{1,0:T(8,128)(2,1)S(1)} collective-permute-done((bf16[512,1024]{1,0:T(8,128)(2,1)}, bf16[512,1024]{1,0:T(8,128)(2,1)S(1)}, u32[]{:S(2)}, u32[]{:S(2)}) %collective-permute-start.11) | collective-permute-done | bytes 1048608 | tf_op jit(solution)/shard_map/ppermute | solution.py:32
  134.8 16.3 %collective-permute-done.23 = bf16[1024,512]{1,0:T(8,128)(2,1)} collective-permute-done((bf16[1024,512]{1,0:T(8,128)(2,1)}, bf16[1024,512]{1,0:T(8,128)(2,1)}, u32[]{:S(2)}, u32[]{:S(2)}) %collective-permute-start.23) | collective-permute-done | bytes 1048608 | tf_op jit(solution)/shard_map/ppermute | solution.py:32
  152.2 21.3 %collective-permute-done.24 = bf16[1024,512]{1,0:T(8,128)(2,1)} collective-permute-done((bf16[1024,512]{1,0:T(8,128)(2,1)}, bf16[1024,512]{1,0:T(8,128)(2,1)}, u32[]{:S(2)}, u32[]{:S(2)}) %collective-permute-start.24) | collective-permute-done | bytes 1048608 | tf_op jit(solution)/shard_map/ppermute | solution.py:32
  176.6 4.1 %shard_map.109 = bf16[512,256]{1,0:T(8,128)(2,1)S(1)} custom-call(s32[16]{0:T(128)S(1)} %pad_add_fusion.ids_ref, s32[1]{0:T(128)} %bitcast.me_ref, bf16[4,64,512]{2,1,0:T(8,128)(2,1)S(1)} %bitcast.43, f32[4,3,512]{2,1,0:T(4,128)S(1)} %copy.25.gate_ref, bf16[4,1280,128]{2,1,0:T(8,128)(2,1)S(1)} %bitcast.42, ...), custom_call_target="tpu_custom_call" | custom-call | flops 6442450944 | bytes 5242880 | tf_op jit(solution)/shard_map/pallas_call | solution.py:270
  182.5 21.1 %collective-permute-start.38 = (bf16[512,512]{1,0:T(8,128)(2,1)S(1)}, bf16[512,512]{1,0:T(8,128)(2,1)S(1)}, u32[]{:S(2)}, u32[]{:S(2)}) collective-permute-start(bf16[512,512]{1,0:T(8,128)(2,1)S(1)} %slice.184), channel_id=1, source_target_pairs={{0,24},{2,26},{4,28},{6,30},{8,0},{10,2},{12,4},{14,6},{16,8},{18,... | collective-permute-start | bytes 1572872 | tf_op jit(solution)/shard_map/ppermute | solution.py:32
  208.7 9.2 %collective-permute-done.38 = bf16[512,512]{1,0:T(8,128)(2,1)S(1)} collective-permute-done((bf16[512,512]{1,0:T(8,128)(2,1)S(1)}, bf16[512,512]{1,0:T(8,128)(2,1)S(1)}, u32[]{:S(2)}, u32[]{:S(2)}) %collective-permute-start.38) | collective-permute-done | bytes 524320 | tf_op jit(solution)/shard_map/ppermute | solution.py:32
  220.0 11.9 %collective-permute-done.15 = bf16[128,2048]{1,0:T(8,128)(2,1)S(1)} collective-permute-done((bf16[128,2048]{1,0:T(8,128)(2,1)S(1)}, bf16[128,2048]{1,0:T(8,128)(2,1)S(1)}, u32[]{:S(2)}, u32[]{:S(2)}) %collective-permute-start.15) | collective-permute-done | bytes 524320 | tf_op jit(solution)/shard_map/ppermute | solution.py:37
  235.5 3.8 %collective-permute-done.16 = bf16[64,2048]{1,0:T(8,128)(2,1)S(1)} collective-permute-done((bf16[64,2048]{1,0:T(8,128)(2,1)S(1)}, bf16[64,2048]{1,0:T(8,128)(2,1)S(1)}, u32[]{:S(2)}, u32[]{:S(2)}) %collective-permute-start.16) | collective-permute-done | bytes 262176 | tf_op jit(solution)/shard_map/ppermute | solution.py:37
  243.8 3.3 %fusion.3 = f32[512,1536]{1,0:T(8,128)S(1)} fusion(bf16[512,1024]{1,0:T(8,128)(2,1)S(1)} %multiply_convert_fusion.1, bf16[1024,512]{1,0:T(8,128)(2,1)} %collective-permute-done.24, bf16[1024,512]{1,0:T(8,128)(2,1)} %collective-permute-done.23, bf16[1024,512]{1,0:T(8,128)(2,1)S(1)} %copy-done.5), kind=kOutput, calls=%fused_computation.10 | convolution fusion | flops 1620049920 | bytes 7340032 | tf_op jit(solution)/shard_map/dot_general | solution.py:157
  251.3 3.3 %convolution_convert_fusion = bf16[512,1536]{1,0:T(8,128)(2,1)S(1)} fusion(bf16[512,1024]{1,0:T(8,128)(2,1)S(1)} %multiply_convert_fusion, bf16[1024,512]{1,0:T(8,128)(2,1)} %collective-permute-done.24, bf16[1024,512]{1,0:T(8,128)(2,1)} %collective-permute-done.23, bf16[1024,512]{1,0:T(8,128)(2,1)S(1)} %copy-done.5), kind=kOutput, calls=%fused_computation.1 | convolution fusion | flops 1620836352 | bytes 5767168 | tf_op jit(solution)/shard_map/dot_general | solution.py:156
  257.9 2.5 collective-permute-done.42
  263.2 4.8 %collective-permute-done.33 = bf16[64,1536]{1,0:T(8,128)(2,1)S(1)} collective-permute-done((bf16[64,1536]{1,0:T(8,128)(2,1)S(1)}, bf16[64,1536]{1,0:T(8,128)(2,1)S(1)}, u32[]{:S(2)}, u32[]{:S(2)}) %collective-permute-start.33) | collective-permute-done | bytes 196640 | tf_op jit(solution)/shard_map/ppermute | solution.py:37
  273.3 6.8 %collective-permute-done.34 = bf16[128,1536]{1,0:T(8,128)(2,1)S(1)} collective-permute-done((bf16[128,1536]{1,0:T(8,128)(2,1)S(1)}, bf16[128,1536]{1,0:T(8,128)(2,1)S(1)}, u32[]{:S(2)}, u32[]{:S(2)}) %collective-permute-start.34) | collective-permute-done | bytes 393248 | tf_op jit(solution)/shard_map/ppermute | solution.py:37
  (199 shorter events, 82.8 us)
Async XLA Ops:
  8.1 13.9 %collective-permute-start = (bf16[1280,128]{0,1:T(8,128)(2,1)}, bf16[1280,128]{0,1:T(8,128)(2,1)S(1)}, u32[]{:S(2)}, u32[]{:S(2)}) collective-permute-start(bf16[1280,128]{0,1:T(8,128)(2,1)} %get-tuple-element.45), channel_id=1, source_target_pairs={{0,8},{2,10},{4,12},{6,14},{8,16},{10,18},{12,20},{14,22},{16,24},... | collective-permute-start | bytes 983048 | tf_op jit(solution)/shard_map/ppermute | solution.py:32
  11.2 16.6 %collective-permute-start.2 = (bf16[1280,128]{0,1:T(8,128)(2,1)}, bf16[1280,128]{0,1:T(8,128)(2,1)S(1)}, u32[]{:S(2)}, u32[]{:S(2)}) collective-permute-start(bf16[1280,128]{0,1:T(8,128)(2,1)} %get-tuple-element.45), channel_id=1, source_target_pairs={{0,24},{2,26},{4,28},{6,30},{8,0},{10,2},{12,4},{14,6},{16,8},{18,... | collective-permute-start | bytes 983048 | tf_op jit(solution)/shard_map/ppermute | solution.py:32
  36.5 56.7 %collective-permute-start.4 = (bf16[4,1280,128]{2,1,0:T(8,128)(2,1)S(1)}, bf16[4,1280,128]{2,1,0:T(8,128)(2,1)}, u32[]{:S(2)}, u32[]{:S(2)}) collective-permute-start(bf16[4,1280,128]{2,1,0:T(8,128)(2,1)S(1)} %bitcast.40), channel_id=1, source_target_pairs={{0,4},{2,6},{4,0},{6,2},{8,12},{10,14},{12,8},{14,10},{16,20},{18,... | collective-permute-start | bytes 3932168 | tf_op jit(solution)/shard_map/ppermute | solution.py:37
  38.3 35.5 %collective-permute-start.8 = (bf16[128,1024]{1,0:T(8,128)(2,1)S(1)}, bf16[128,1024]{1,0:T(8,128)(2,1)S(1)}, u32[]{:S(2)}, u32[]{:S(2)}) collective-permute-start(bf16[128,1024]{1,0:T(8,128)(2,1)S(1)} %copy-done.7), channel_id=1, source_target_pairs={{0,4},{2,6},{4,0},{6,2},{8,12},{10,14},{12,8},{14,10},{16,20},{18,... | collective-permute-start | bytes 786440 | tf_op jit(solution)/shard_map/ppermute | solution.py:37
  38.6 38.6 %collective-permute-start.9 = (bf16[128,1024]{1,0:T(8,128)(2,1)S(1)}, bf16[128,1024]{1,0:T(8,128)(2,1)S(1)}, u32[]{:S(2)}, u32[]{:S(2)}) collective-permute-start(bf16[128,1024]{1,0:T(8,128)(2,1)S(1)} %get-tuple-element.25), channel_id=1, source_target_pairs={{0,6},{2,4},{4,2},{6,0},{8,14},{10,12},{12,10},{14,8},{16,22},{18,... | collective-permute-start | bytes 786440 | tf_op jit(solution)/shard_map/ppermute | solution.py:37
  77.9 28.1 %collective-permute-start.10 = (bf16[512,1024]{1,0:T(8,128)(2,1)}, bf16[512,1024]{1,0:T(8,128)(2,1)S(1)}, u32[]{:S(2)}, u32[]{:S(2)}) collective-permute-start(bf16[512,1024]{1,0:T(8,128)(2,1)} %constant_dynamic-update-slice_fusion.30), channel_id=1, source_target_pairs={{0,8},{2,10},{4,12},{6,14},{8,16},{10,18},{12,20},{14,22},{16,24},... | collective-permute-start | bytes 3145736 | tf_op jit(solution)/shard_map/ppermute | solution.py:32
  79.3 48.1 %collective-permute-start.11 = (bf16[512,1024]{1,0:T(8,128)(2,1)}, bf16[512,1024]{1,0:T(8,128)(2,1)S(1)}, u32[]{:S(2)}, u32[]{:S(2)}) collective-permute-start(bf16[512,1024]{1,0:T(8,128)(2,1)} %constant_dynamic-update-slice_fusion.30), channel_id=1, source_target_pairs={{0,24},{2,26},{4,28},{6,30},{8,0},{10,2},{12,4},{14,6},{16,8},{18,... | collective-permute-start | bytes 3145736 | tf_op jit(solution)/shard_map/ppermute | solution.py:32
  85.4 12.5 %collective-permute-start.22 = (bf16[1024,128]{1,0:T(8,128)(2,1)}, bf16[1024,128]{1,0:T(8,128)(2,1)}, u32[]{:S(2)}, u32[]{:S(2)}) collective-permute-start(bf16[1024,128]{1,0:T(8,128)(2,1)} %get-tuple-element.21), channel_id=1, source_target_pairs={{0,6},{2,4},{4,2},{6,0},{8,14},{10,12},{12,10},{14,8},{16,22},{18,... | collective-permute-start | bytes 786440 | tf_op jit(solution)/shard_map/ppermute | solution.py:37
  93.2 82.8 %collective-permute-start.5 = (bf16[4,1280,128]{2,1,0:T(8,128)(2,1)S(1)}, bf16[4,1280,128]{2,1,0:T(8,128)(2,1)}, u32[]{:S(2)}, u32[]{:S(2)}) collective-permute-start(bf16[4,1280,128]{2,1,0:T(8,128)(2,1)S(1)} %bitcast.41), channel_id=1, source_target_pairs={{0,2},{2,0},{4,6},{6,4},{8,10},{10,8},{12,14},{14,12},{16,18},{18,... | collective-permute-start | bytes 3932168 | tf_op jit(solution)/shard_map/ppermute | solution.py:37
  93.2 83.4 %collective-permute-start.6 = (bf16[4,1280,128]{2,1,0:T(8,128)(2,1)}, bf16[4,1280,128]{2,1,0:T(8,128)(2,1)}, u32[]{:S(2)}, u32[]{:S(2)}) collective-permute-start(bf16[4,1280,128]{2,1,0:T(8,128)(2,1)} %collective-permute-done.4.refs_1_), channel_id=1, source_target_pairs={{0,2},{2,0},{4,6},{6,4},{8,10},{10,8},{12,14},{14,12},{16,18},{18,... | collective-permute-start | bytes 3932168 | tf_op jit(solution)/shard_map/ppermute | solution.py:37
  97.9 84.6 %collective-permute-start.13 = (bf16[512,2048]{1,0:T(8,128)(2,1)}, bf16[512,2048]{1,0:T(8,128)(2,1)}, u32[]{:S(2)}, u32[]{:S(2)}) collective-permute-start(bf16[512,2048]{1,0:T(8,128)(2,1)} %param.18), channel_id=1, source_target_pairs={{0,1},{1,0},{2,3},{3,2},{4,5},{5,4},{6,7},{7,6},{8,9},{9,8},{10,11... | collective-permute-start | bytes 6291464 | tf_op jit(solution)/shard_map/ppermute | solution.py:32
  106.0 45.1 %collective-permute-start.23 = (bf16[1024,512]{1,0:T(8,128)(2,1)}, bf16[1024,512]{1,0:T(8,128)(2,1)}, u32[]{:S(2)}, u32[]{:S(2)}) collective-permute-start(bf16[1024,512]{1,0:T(8,128)(2,1)} %constant_dynamic-update-slice_fusion.22), channel_id=1, source_target_pairs={{0,8},{2,10},{4,12},{6,14},{8,16},{10,18},{12,20},{14,22},{16,24},... | collective-permute-start | bytes 3145736 | tf_op jit(solution)/shard_map/ppermute | solution.py:32
  127.4 46.0 %collective-permute-start.24 = (bf16[1024,512]{1,0:T(8,128)(2,1)}, bf16[1024,512]{1,0:T(8,128)(2,1)}, u32[]{:S(2)}, u32[]{:S(2)}) collective-permute-start(bf16[1024,512]{1,0:T(8,128)(2,1)} %constant_dynamic-update-slice_fusion.22), channel_id=1, source_target_pairs={{0,24},{2,26},{4,28},{6,30},{8,0},{10,2},{12,4},{14,6},{16,8},{18,... | collective-permute-start | bytes 3145736 | tf_op jit(solution)/shard_map/ppermute | solution.py:32
  151.1 68.7 %collective-permute-start.18 = (bf16[256,1024]{1,0:T(8,128)(2,1)S(1)}, bf16[256,1024]{1,0:T(8,128)(2,1)S(1)}, u32[]{:S(2)}, u32[]{:S(2)}) collective-permute-start(bf16[256,1024]{1,0:T(8,128)(2,1)S(1)} %slice.166), channel_id=1, source_target_pairs={{0,8},{2,10},{4,12},{6,14},{8,16},{10,18},{12,20},{14,22},{16,24},... | collective-permute-start | bytes 1572872 | tf_op jit(solution)/shard_map/ppermute | solution.py:32
  173.5 46.4 %collective-permute-start.19 = (bf16[256,1024]{1,0:T(8,128)(2,1)S(1)}, bf16[256,1024]{1,0:T(8,128)(2,1)S(1)}, u32[]{:S(2)}, u32[]{:S(2)}) collective-permute-start(bf16[256,1024]{1,0:T(8,128)(2,1)S(1)} %slice.167), channel_id=1, source_target_pairs={{0,24},{2,26},{4,28},{6,30},{8,0},{10,2},{12,4},{14,6},{16,8},{18,... | collective-permute-start | bytes 1572872 | tf_op jit(solution)/shard_map/ppermute | solution.py:32
  176.0 31.2 %collective-permute-start.37 = (bf16[512,512]{1,0:T(8,128)(2,1)S(1)}, bf16[512,512]{1,0:T(8,128)(2,1)S(1)}, u32[]{:S(2)}, u32[]{:S(2)}) collective-permute-start(bf16[512,512]{1,0:T(8,128)(2,1)S(1)} %slice.183), channel_id=1, source_target_pairs={{0,8},{2,10},{4,12},{6,14},{8,16},{10,18},{12,20},{14,22},{16,24},... | collective-permute-start | bytes 1572872 | tf_op jit(solution)/shard_map/ppermute | solution.py:32
  180.8 22.8 %collective-permute-start.12 = (bf16[512,128]{1,0:T(8,128)(2,1)S(1)}, bf16[512,128]{1,0:T(8,128)(2,1)S(1)}, u32[]{:S(2)}, u32[]{:S(2)}) collective-permute-start(bf16[512,128]{1,0:T(8,128)(2,1)S(1)} %constant_dynamic-slice_fusion.3), channel_id=1, source_target_pairs={{0,1},{1,0},{2,3},{3,2},{4,5},{5,4},{6,7},{7,6},{8,9},{9,8},{10,11... | collective-permute-start | bytes 393224 | tf_op jit(solution)/shard_map/ppermute | solution.py:32
  182.5 35.5 %collective-permute-start.38 = (bf16[512,512]{1,0:T(8,128)(2,1)S(1)}, bf16[512,512]{1,0:T(8,128)(2,1)S(1)}, u32[]{:S(2)}, u32[]{:S(2)}) collective-permute-start(bf16[512,512]{1,0:T(8,128)(2,1)S(1)} %slice.184), channel_id=1, source_target_pairs={{0,24},{2,26},{4,28},{6,30},{8,0},{10,2},{12,4},{14,6},{16,8},{18,... | collective-permute-start | bytes 1572872 | tf_op jit(solution)/shard_map/ppermute | solution.py:32
  206.5 28.9 %collective-permute-start.25 = (bf16[128,2048]{1,0:T(8,128)(2,1)S(1)}, bf16[128,2048]{1,0:T(8,128)(2,1)S(1)}, u32[]{:S(2)}, u32[]{:S(2)}) collective-permute-start(bf16[128,2048]{1,0:T(8,128)(2,1)S(1)} %get-tuple-element.10), channel_id=1, source_target_pairs={{0,2},{2,0},{4,6},{6,4},{8,10},{10,8},{12,14},{14,12},{16,18},{18,... | collective-permute-start | bytes 1572872 | tf_op jit(solution)/shard_map/ppermute | solution.py:37
  207.2 26.4 %collective-permute-start.14 = (bf16[128,2048]{1,0:T(8,128)(2,1)S(1)}, bf16[128,2048]{1,0:T(8,128)(2,1)S(1)}, u32[]{:S(2)}, u32[]{:S(2)}) collective-permute-start(bf16[128,2048]{1,0:T(8,128)(2,1)S(1)} %get-tuple-element.10), channel_id=1, source_target_pairs={{0,1},{1,0},{2,3},{3,2},{4,5},{5,4},{6,7},{7,6},{8,9},{9,8},{10,11... | collective-permute-start | bytes 1572872 | tf_op jit(solution)/shard_map/ppermute | solution.py:37
  218.0 13.8 %collective-permute-start.15 = (bf16[128,2048]{1,0:T(8,128)(2,1)S(1)}, bf16[128,2048]{1,0:T(8,128)(2,1)S(1)}, u32[]{:S(2)}, u32[]{:S(2)}) collective-permute-start(bf16[128,2048]{1,0:T(8,128)(2,1)S(1)} %get-tuple-element.10), channel_id=1, source_target_pairs={{0,4},{2,6},{4,0},{6,2},{8,12},{10,14},{12,8},{14,10},{16,20},{18,... | collective-permute-start | bytes 1572872 | tf_op jit(solution)/shard_map/ppermute | solution.py:37
  234.9 13.0 %collective-permute-start.26 = (bf16[128,2048]{1,0:T(8,128)(2,1)S(1)}, bf16[128,2048]{1,0:T(8,128)(2,1)S(1)}, u32[]{:S(2)}, u32[]{:S(2)}) collective-permute-start(bf16[128,2048]{1,0:T(8,128)(2,1)S(1)} %collective-permute-done.14), channel_id=1, source_target_pairs={{0,2},{2,0},{4,6},{6,4},{8,10},{10,8},{12,14},{14,12},{16,18},{18,... | collective-permute-start | bytes 1572872 | tf_op jit(solution)/shard_map/ppermute | solution.py:37
  234.9 13.0 %collective-permute-start.27 = (bf16[128,2048]{1,0:T(8,128)(2,1)S(1)}, bf16[128,2048]{1,0:T(8,128)(2,1)S(1)}, u32[]{:S(2)}, u32[]{:S(2)}) collective-permute-start(bf16[128,2048]{1,0:T(8,128)(2,1)S(1)} %collective-permute-done.15), channel_id=1, source_target_pairs={{0,2},{2,0},{4,6},{6,4},{8,10},{10,8},{12,14},{14,12},{16,18},{18,... | collective-permute-start | bytes 1572872 | tf_op jit(solution)/shard_map/ppermute | solution.py:37
  255.3 26.0 %collective-permute-start.39 = (bf16[128,512]{1,0:T(8,128)(2,1)S(1)}, bf16[128,512]{1,0:T(8,128)(2,1)S(1)}, u32[]{:S(2)}, u32[]{:S(2)}) collective-permute-start(bf16[128,512]{1,0:T(8,128)(2,1)S(1)} %get-tuple-element.31), channel_id=1, source_target_pairs={{0,2},{2,0},{4,6},{6,4},{8,10},{10,8},{12,14},{14,12},{16,18},{18,... | collective-permute-start | bytes 393224 | tf_op jit(solution)/shard_map/ppermute | solution.py:37
  (32 other events, 407.4 us)
